TPU v7x, 32 devices: a whole 2x2x4 slice. The times are simulated.
32 devices in a mesh: fs: 16 (over z, y, x), tp: 2 (over core).
Axes of the slice: x: 2, y: 2, z: 4, core: 2. Of those that a mesh axis runs over, the one named last changes fastest.
Arguments:
- tokens: bfloat16 [8192, 2048], P('fs', 'tp'), may hold values from -24 to 24
- u_weight: bfloat16 [2048, 1024], P('fs', 'tp'), may hold values from -0.125 to 0.125
- v_weight: bfloat16 [2048, 1024], P('fs', 'tp'), may hold values from -0.125 to 0.125
- sg_gain: float32 [1024], P('tp'), may hold values from 0.1 to 1.9
- spatial_weight: bfloat16 [8, 128, 128], P('tp'), may hold values from -0.5 to 0.5
- spatial_bias: float32 [8, 128], P('tp'), may hold values from 0.1 to 1.9
- out_weight: bfloat16 [1024, 2048], P('tp', 'fs'), may hold values from -0.1875 to 0.1875
- gain_one: float32 [2048], P('tp'), may hold values from 0.1 to 1.9
- gate_weight: bfloat16 [2048, 5632], P('fs', 'tp'), may hold values from -0.125 to 0.125
- up_weight: bfloat16 [2048, 5632], P('fs', 'tp'), may hold values from -0.125 to 0.125
- down_weight: bfloat16 [5632, 2048], P('tp', 'fs'), may hold values from -0.078125 to 0.078125
- gain_two: float32 [2048], P('tp'), may hold values from 0.1 to 1.9
Outputs:
- layer_out: bfloat16 [8192, 2048], P('fs', 'tp')
All inputs are finite; a program needn't handle non-finite values.
Results may differ from a plain program's by a relative error of at most 0.014.
Values may be sent and summed in bfloat16 or wider, within the bound.
A program may use at most 128 MiB of HBM per device.

v0:
```python
import jax
import jax.numpy as jnp
from jax import lax
from jax.sharding import PartitionSpec as P

EPS = 1e-05
ALPHA = 2.0**0.25


def add_rows(left, piece):
    return jnp.dot(left, piece, preferred_element_type=jnp.float32)


def scaled_rows(vals, sums, gain, count):
    mean = sums[0][:, None] / count
    square = sums[1][:, None] / count
    return (vals - mean) * lax.rsqrt(square - mean * mean + EPS) * gain[None, :]


def on_device(
    tokens,
    u_weight,
    v_weight,
    sg_gain,
    spatial_weight,
    spatial_bias,
    out_weight,
    gain_one,
    gate_weight,
    up_weight,
    down_weight,
    gain_two,
):
    parts = lax.axis_size("tp")
    whole = lax.all_gather(tokens, "tp", axis=1, tiled=True)
    rows = whole.shape[0]
    width_sg = u_weight.shape[1]

    def add_one(piece):
        return add_rows(whole, piece)

    pre_u = add_one(lax.all_gather(u_weight, "fs", axis=0, tiled=True))
    pre_v = add_one(lax.all_gather(v_weight, "fs", axis=0, tiled=True))
    gated = jax.nn.gelu(pre_u)
    valued = jax.nn.gelu(pre_v)
    stats = lax.psum((jnp.sum(valued, axis=1), jnp.sum(valued * valued, axis=1)), "tp")
    normed = scaled_rows(valued, stats, sg_gain, width_sg * parts).astype(jnp.bfloat16)
    groups_here = spatial_weight.shape[0]
    block = spatial_weight.shape[1]
    group_width = width_sg // groups_here
    shaped = normed.reshape(rows // block, block, groups_here, group_width)
    lower = jnp.tril(jnp.ones((block, block), jnp.bool_))
    masked = jnp.where(lower[None], spatial_weight, jnp.zeros_like(spatial_weight))
    mixed = jnp.einsum("gij,njgd->nigd", masked, shaped, preferred_element_type=jnp.float32)
    mixed = mixed + spatial_bias.T[None, :, :, None]
    gated_out = (gated * mixed.reshape(rows, width_sg)).astype(jnp.bfloat16)
    terms = jnp.dot(
        gated_out,
        lax.all_gather(out_weight, "fs", axis=1, tiled=True),
        preferred_element_type=jnp.float32,
    )
    mix = lax.psum_scatter(terms.astype(jnp.bfloat16), "tp", scatter_dimension=1, tiled=True)
    resid = ALPHA * tokens.astype(jnp.float32) + mix.astype(jnp.float32)
    first_sums = lax.psum((jnp.sum(resid, axis=1), jnp.sum(resid * resid, axis=1)), "tp")
    first = scaled_rows(resid, first_sums, gain_one, resid.shape[1] * parts).astype(jnp.bfloat16)
    whole_first = lax.all_gather(first, "tp", axis=1, tiled=True)

    def add_first(piece):
        return add_rows(whole_first, piece)

    gate = add_first(lax.all_gather(gate_weight, "fs", axis=0, tiled=True))
    upper = add_first(lax.all_gather(up_weight, "fs", axis=0, tiled=True))
    hidden = (jax.nn.silu(gate) * upper).astype(jnp.bfloat16)
    ffn_terms = jnp.dot(
        hidden,
        lax.all_gather(down_weight, "fs", axis=1, tiled=True),
        preferred_element_type=jnp.float32,
    )
    ffn = lax.psum_scatter(ffn_terms.astype(jnp.bfloat16), "tp", scatter_dimension=1, tiled=True)
    second = ALPHA * first.astype(jnp.float32) + ffn.astype(jnp.float32)
    last_sums = lax.psum((jnp.sum(second, axis=1), jnp.sum(second * second, axis=1)), "tp")
    return scaled_rows(second, last_sums, gain_two, second.shape[1] * parts).astype(jnp.bfloat16)


def solution(mesh):
    return jax.shard_map(
        on_device,
        mesh=mesh,
        in_specs=(
            P("fs", "tp"),
            P("fs", "tp"),
            P("fs", "tp"),
            P("tp"),
            P("tp", None, None),
            P("tp", None),
            P("tp", "fs"),
            P("tp"),
            P("fs", "tp"),
            P("fs", "tp"),
            P("tp", "fs"),
            P("tp"),
        ),
        out_specs=P("fs", "tp"),
        check_vma=False,
    )
```

profile of v0, /device:TPU:0, one launch (start us, length us, event | category | flops | bytes accessed | tf_op | source)
XLA Modules:
  0.0 759.9 jit_solution(2212430606449240204)
XLA Ops:
  6.5 0.7 all-gather.9.cloned.1.call-update
  9.4 12.8 %all-gather.9.cloned.1.call-done = bf16[512,2048]{1,0:T(8,128)(2,1)} async-done(((bf16[512,1024]{1,0:T(8,128)(2,1)}), bf16[512,2048]{1,0:T(8,128)(2,1)}) %all-gather.9.cloned.1.call-update) | async-done | bytes 2097168 | tf_op jit(solution)/shard_map/all_gather | solution.py:35
  22.2 64.4 %all-gather.13.cloned.1.call-done = bf16[2048,512]{1,0:T(8,128)(2,1)} async-done(((bf16[128,512]{1,0:T(8,128)(2,1)}), bf16[2048,512]{1,0:T(8,128)(2,1)}) %all-gather.13.cloned.1.call-update) | async-done | bytes 2097168 | tf_op jit(solution)/shard_map/all_gather | solution.py:43
  86.6 3.8 fusion.35
  90.4 2.6 all-reduce.2
  94.4 54.1 %all-gather.11.cloned.1.call-done = bf16[2048,512]{1,0:T(8,128)(2,1)} async-done(((bf16[128,512]{1,0:T(8,128)(2,1)}), bf16[2048,512]{1,0:T(8,128)(2,1)}) %all-gather.11.cloned.1.call-update) | async-done | bytes 2097168 | tf_op jit(solution)/shard_map/all_gather | solution.py:42
  148.5 64.3 %all-gather.15.cloned.1.call-done = bf16[512,2048]{1,0:T(8,128)(2,1)} async-done(((bf16[512,128]{1,0:T(8,128)(2,1)}), bf16[512,2048]{1,0:T(8,128)(2,1)}) %all-gather.15.cloned.1.call-update) | async-done | bytes 2097168 | tf_op jit(solution)/shard_map/all_gather | solution.py:59
  212.9 6.8 convolution_convert_fusion.1
  219.7 7.9 %reduce-scatter.3.cloned.1.call-done = bf16[512,1024]{1,0:T(8,128)(2,1)} async-done(((bf16[512,2048]{1,0:T(8,128)(2,1)}), bf16[512,1024]{1,0:T(8,128)(2,1)}) %reduce-scatter.3.cloned.1.call-update) | async-done | bytes 1048592 | tf_op jit(solution)/shard_map/reduce_scatter | solution.py:62
  227.6 1.9 fusion
  229.5 2.5 all-reduce.1
  232.0 1.5 multiply_convert_fusion.2
  233.6 0.7 all-gather.19.cloned.1.call-update
  234.4 0.7 all-gather.21.cloned.1.call-update
  236.1 9.5 %all-gather.17.cloned.1.call-done = bf16[512,2048]{1,0:T(8,128)(2,1)} async-done(((bf16[512,1024]{1,0:T(8,128)(2,1)}), bf16[512,2048]{1,0:T(8,128)(2,1)}) %all-gather.17.cloned.1.call-update) | async-done | bytes 2097168 | tf_op jit(solution)/shard_map/all_gather | solution.py:66
  245.6 145.4 %all-gather.19.cloned.1.call-done = bf16[2048,2816]{1,0:T(8,128)(2,1)} async-done(((bf16[128,2816]{1,0:T(8,128)(2,1)}), bf16[2048,2816]{1,0:T(8,128)(2,1)}) %all-gather.19.cloned.1.call-update) | async-done | bytes 11534352 | tf_op jit(solution)/shard_map/all_gather | solution.py:71
  391.0 12.5 %fusion.38 = f32[512,2816]{1,0:T(8,128)} fusion(bf16[512,2048]{1,0:T(8,128)(2,1)} %all-gather.17.cloned.1.call-done, bf16[2048,2816]{1,0:T(8,128)(2,1)} %all-gather.19.cloned.1.call-done), kind=kOutput, calls=%fused_computation.57 | convolution fusion | flops 5905580032 | bytes 19398656 | tf_op jit(solution)/shard_map/dot_general | solution.py:11
  403.5 129.9 %all-gather.21.cloned.1.call-done = bf16[2048,2816]{1,0:T(8,128)(2,1)} async-done(((bf16[128,2816]{1,0:T(8,128)(2,1)}), bf16[2048,2816]{1,0:T(8,128)(2,1)}) %all-gather.21.cloned.1.call-update) | async-done | bytes 11534352 | tf_op jit(solution)/shard_map/all_gather | solution.py:72
  533.4 183.0 %all-gather.23.cloned.1.call-done = bf16[2816,2048]{1,0:T(8,128)(2,1)} async-done(((bf16[2816,128]{1,0:T(8,128)(2,1)}), bf16[2816,2048]{1,0:T(8,128)(2,1)}) %all-gather.23.cloned.1.call-update) | async-done | bytes 11534352 | tf_op jit(solution)/shard_map/all_gather | solution.py:76
  716.4 22.8 %convolution_convert_fusion = bf16[512,2048]{1,0:T(8,128)(2,1)} fusion(bf16[2816,2048]{1,0:T(8,128)(2,1)} %all-gather.23.cloned.1.call-done, f32[512,2816]{1,0:T(8,128)} %fusion.38, bf16[512,2048]{1,0:T(8,128)(2,1)S(1)} %copy-done.9, bf16[2048,2816]{1,0:T(8,128)(2,1)} %all-gather.21.cloned.1.call-done), kind=kOutput, calls=%fused_computation.1 | convolution fusion | flops 11820859392 | bytes 33030144 | tf_op jit(solution)/shard_map/dot_general | solution.py:74
  739.2 8.0 %reduce-scatter.5.cloned.1.call-done = bf16[512,1024]{1,0:T(8,128)(2,1)} async-done(((bf16[512,2048]{1,0:T(8,128)(2,1)}), bf16[512,1024]{1,0:T(8,128)(2,1)}) %reduce-scatter.5.cloned.1.call-update) | async-done | bytes 1048592 | tf_op jit(solution)/shard_map/reduce_scatter | solution.py:79
  747.1 1.9 fusion.1
  749.0 2.5 all-reduce
  751.5 1.5 multiply_convert_fusion.1
  (45 shorter events, 4.6 us)
Async XLA Ops:
  6.5 15.7 %all-gather.9.cloned.1.call-start = ((), (), s32[]{:S(2)}) async-start(), calls=%async_computation.2 | async-start | bytes 3145728 | tf_op jit(solution)/shard_map/all_gather | solution.py:35
  7.3 79.3 %all-gather.13.cloned.1.call-start = ((), (), s32[]{:S(2)}) async-start(), calls=%async_computation.4 | async-start | bytes 2228224 | tf_op jit(solution)/shard_map/all_gather | solution.py:43
  8.0 140.5 %all-gather.11.cloned.1.call-start = ((), (), s32[]{:S(2)}) async-start(), calls=%async_computation.3 | async-start | bytes 2228224 | tf_op jit(solution)/shard_map/all_gather | solution.py:42
  8.7 204.1 %all-gather.15.cloned.1.call-start = ((), (), s32[]{:S(2)}) async-start(), calls=%async_computation.5 | async-start | bytes 2228224 | tf_op jit(solution)/shard_map/all_gather | solution.py:59
  9.3 218.3 %reduce-scatter.3.cloned.1.call-start = ((), (), s32[]{:S(2)}) async-start(), calls=%async_computation.6 | async-start | bytes 3145728 | tf_op jit(solution)/shard_map/reduce_scatter | solution.py:62
  9.4 83.7 %copy-start.7 = (f32[512]{0:T(512)S(1)}, f32[512]{0:T(512)}, u32[]{:S(2)}) copy-start(f32[512]{0:T(512)} %param.15) | copy-start | bytes 6148
  90.4 3.2 copy-start.4
  90.4 3.2 copy-start.8
  219.7 8.0 %copy-start.1 = (bf16[512,1024]{1,0:T(8,128)(2,1)S(1)}, bf16[512,1024]{1,0:T(8,128)(2,1)}, u32[]{:S(2)}) copy-start(bf16[512,1024]{1,0:T(8,128)(2,1)} %param.12) | copy-start | bytes 3145732
  219.7 12.4 %copy-start.5 = (f32[1024]{0:T(1024)S(1)}, f32[1024]{0:T(1024)}, u32[]{:S(2)}) copy-start(f32[1024]{0:T(1024)} %param.19) | copy-start | bytes 12292
  219.7 25.9 %all-gather.17.cloned.1.call-start = ((), (), s32[]{:S(2)}) async-start(), calls=%async_computation.7 | async-start | bytes 3145728 | tf_op jit(solution)/shard_map/all_gather | solution.py:66
  227.6 4.4 copy-start.2
  233.6 157.4 %all-gather.19.cloned.1.call-start = ((), (), s32[]{:S(2)}) async-start(), calls=%async_computation.8 | async-start | bytes 12255232 | tf_op jit(solution)/shard_map/all_gather | solution.py:71
  234.3 299.1 %all-gather.21.cloned.1.call-start = ((), (), s32[]{:S(2)}) async-start(), calls=%async_computation.9 | async-start | bytes 12255232 | tf_op jit(solution)/shard_map/all_gather | solution.py:72
  235.1 481.3 %all-gather.23.cloned.1.call-start = ((), (), s32[]{:S(2)}) async-start(), calls=%async_computation.10 | async-start | bytes 12255232 | tf_op jit(solution)/shard_map/all_gather | solution.py:76
  235.8 511.3 %reduce-scatter.5.cloned.1.call-start = ((), (), s32[]{:S(2)}) async-start(), calls=%async_computation.11 | async-start | bytes 3145728 | tf_op jit(solution)/shard_map/reduce_scatter | solution.py:79
  245.6 470.8 %copy-start.9 = (bf16[512,2048]{1,0:T(8,128)(2,1)S(1)}, bf16[512,2048]{1,0:T(8,128)(2,1)}, u32[]{:S(2)}) copy-start(bf16[512,2048]{1,0:T(8,128)(2,1)} %all-gather.17.cloned.1.call-done) | copy-start | bytes 6291460
  739.1 8.0 %copy-start = (bf16[512,1024]{1,0:T(8,128)(2,1)S(1)}, bf16[512,1024]{1,0:T(8,128)(2,1)}, u32[]{:S(2)}) copy-start(bf16[512,1024]{1,0:T(8,128)(2,1)} %multiply_convert_fusion.2) | copy-start | bytes 3145732
  739.1 12.4 %copy-start.6 = (f32[1024]{0:T(1024)S(1)}, f32[1024]{0:T(1024)}, u32[]{:S(2)}) copy-start(f32[1024]{0:T(1024)} %param.23) | copy-start | bytes 12292
  747.1 4.4 copy-start.3
Sparse Core Ops, SparseCore 0:
  8.9 13.2 all-gather.8
  25.0 61.5 all-gather.12
  89.3 59.1 all-gather.10
  151.1 61.7 all-gather.14
  219.8 7.7 reduce-scatter.2
  233.7 11.8 all-gather.16
  248.3 142.5 all-gather.18
  393.7 139.6 all-gather.20
  536.1 180.2 all-gather.22
  739.3 7.7 reduce-scatter.4
where the time goes:
time: 760 us
  waiting for transfers between devices  684 us (90%)
  matrix products  46.3 us (6%)
  between operations  13.6 us (2%)
    all_gather x1, waiting for transfers between devices, on_device(): lax.all_gather(down_weight, 'fs', axis=1, tiled=True)  183 us
    all_gather x1, waiting for transfers between devices, on_device(): gate = add_first(lax.all_gather(gate_weight, 'fs', axis=0, tiled=True))  145 us
    all_gather x1, waiting for transfers between devices, on_device(): upper = add_first(lax.all_gather(up_weight, 'fs', axis=0, tiled=True))  130 us
    all_gather x1, waiting for transfers between devices, on_device(): pre_v = add_one(lax.all_gather(v_weight, 'fs', axis=0, tiled=True))  64.4 us
    all_gather x1, waiting for transfers between devices, on_device(): lax.all_gather(out_weight, 'fs', axis=1, tiled=True)  64.3 us
    all_gather x1, waiting for transfers between devices, on_device(): pre_u = add_one(lax.all_gather(u_weight, 'fs', axis=0, tiled=True))  54.1 us
    dot_general x1, matrix products, on_device(): jnp.dot(hidden, lax.all_gather(down_weight, 'fs', axis=1, tiled=True), pr...  22.8 us
    dot_general x2, matrix products, add_rows(): return jnp.dot(left, piece, preferred_element_type=jnp.float32)  16.3 us
  transfers between devices with their start and end apart: 10, of which 10 were waited for; matrix products, arithmetic and copies ran while one was open for 2% of the time, Pallas kernels for 0%

commit v1 on v0

--- a/solution.py
+++ b/solution.py
@@ -31,6 +31,13 @@
     down_weight,
     gain_two,
 ):
+
+    def state_the_stops_all(peer_axis, in_array):
+        a_now = jnp.stack(lax.axis_size(peer_axis) * [in_array])
+        current_arr = lax.all_to_all(a_now, peer_axis, 0, 0)
+        response = jnp.concatenate(current_arr, 0)
+        return response
+
     parts = lax.axis_size("tp")
     whole = lax.all_gather(tokens, "tp", axis=1, tiled=True)
     rows = whole.shape[0]
@@ -39,7 +46,7 @@
     def add_one(piece):
         return add_rows(whole, piece)
 
-    pre_u = add_one(lax.all_gather(u_weight, "fs", axis=0, tiled=True))
+    pre_u = add_one(state_the_stops_all("fs", u_weight))
     pre_v = add_one(lax.all_gather(v_weight, "fs", axis=0, tiled=True))
     gated = jax.nn.gelu(pre_u)
     valued = jax.nn.gelu(pre_v)

time: 760 us -> 709 us (0.933)
  waiting for transfers between devices: 684 us -> 618 us
  starting transfers between devices: 0.53 us -> 8.84 us
    all_gather x1 -> x0, waiting for transfers between devices: 54.1 us -> none  [on_device(): pre_u = add_one(lax.all_gather(u_weight, 'fs', axis=0, tiled=True))]
    all_gather x1, waiting for transfers between devices: 64.3 us -> 52 us  [on_device(): lax.all_gather(out_weight, 'fs', axis=1, tiled=True)]
    all_gather x1, waiting for transfers between devices: 64.4 us -> 75.7 us  [on_device(): pre_v = add_one(lax.all_gather(v_weight, 'fs', axis=0, tiled=True))]
    all_gather x1, waiting for transfers between devices: 12.8 us -> 2.58 us  [on_device(): whole = lax.all_gather(tokens, 'tp', axis=1, tiled=True)]
    all_to_all x0 -> x1, starting transfers between devices: none -> 8.34 us  [state_the_stops_all(): current_arr = lax.all_to_all(a_now, peer_axis, 0, 0)]
  transfers between devices with their start and end apart: 10 -> 10, of which waited for: 10 -> 9; matrix products, arithmetic and copies ran while one was open for 2% -> 4% of each run, Pallas kernels for 0% -> 0%
where the time goes in v1:
time: 709 us
  waiting for transfers between devices  618 us (87%)
  matrix products  47.7 us (7%)
  between operations  13.3 us (2%)
  starting transfers between devices  8.84 us (1%)
  other arithmetic  8.5 us (1%)
  blocking collectives  7.52 us (1%)
    all_gather x1, waiting for transfers between devices, on_device(): lax.all_gather(down_weight, 'fs', axis=1, tiled=True)  183 us
    all_gather x1, waiting for transfers between devices, on_device(): gate = add_first(lax.all_gather(gate_weight, 'fs', axis=0, tiled=True))  145 us
    all_gather x1, waiting for transfers between devices, on_device(): upper = add_first(lax.all_gather(up_weight, 'fs', axis=0, tiled=True))  130 us
    all_gather x1, waiting for transfers between devices, on_device(): pre_v = add_one(lax.all_gather(v_weight, 'fs', axis=0, tiled=True))  75.7 us
    all_gather x1, waiting for transfers between devices, on_device(): lax.all_gather(out_weight, 'fs', axis=1, tiled=True)  52 us
    dot_general x1, matrix products, on_device(): jnp.dot(hidden, lax.all_gather(down_weight, 'fs', axis=1, tiled=True), pr...  22.8 us
    dot_general x2, matrix products, add_rows(): return jnp.dot(left, piece, preferred_element_type=jnp.float32)  17.1 us
  transfers between devices with their start and end apart: 10, of which 9 were waited for; matrix products, arithmetic and copies ran while one was open for 4% of the time, Pallas kernels for 0%

profile of v1, /device:TPU:0, one launch (start us, length us, event | category | flops | bytes accessed | tf_op | source)
XLA Modules:
  0.0 708.5 jit_solution(5176097042439545202)
XLA Ops:
  8.0 2.4 stack.2
  10.5 8.3 %all-to-all-start = ((bf16[16,128,512]{2,1,0:T(8,128)(2,1)}), bf16[16,128,512]{2,1,0:T(8,128)(2,1)S(1)}, u32[]{:S(2)}, u32[]{:S(2)}) async-start(bf16[16,128,512]{2,1,0:T(8,128)(2,1)} %stack.2), calls=%async_computation | async-start | bytes 4194304 | tf_op jit(solution)/shard_map/all_to_all | solution.py:37
  19.6 2.6 all-gather.8.cloned.1.call-done
  22.2 75.7 %all-gather.10.cloned.1.call-done = bf16[2048,512]{1,0:T(8,128)(2,1)} async-done(((bf16[128,512]{1,0:T(8,128)(2,1)}), bf16[2048,512]{1,0:T(8,128)(2,1)}) %all-gather.10.cloned.1.call-update) | async-done | bytes 2097168 | tf_op jit(solution)/shard_map/all_gather | solution.py:50
  97.9 4.6 fusion.35
  102.5 2.6 all-reduce.2
  105.1 1.7 multiply_convert_fusion.3
  107.7 1.4 fusion.2
  110.4 52.0 %all-gather.12.cloned.1.call-done = bf16[512,2048]{1,0:T(8,128)(2,1)} async-done(((bf16[512,128]{1,0:T(8,128)(2,1)}), bf16[512,2048]{1,0:T(8,128)(2,1)}) %all-gather.12.cloned.1.call-update) | async-done | bytes 2097168 | tf_op jit(solution)/shard_map/all_gather | solution.py:66
  162.3 6.5 convolution_convert_fusion.1
  168.9 7.9 %reduce-scatter.3.cloned.1.call-done = bf16[512,1024]{1,0:T(8,128)(2,1)} async-done(((bf16[512,2048]{1,0:T(8,128)(2,1)}), bf16[512,1024]{1,0:T(8,128)(2,1)}) %reduce-scatter.3.cloned.1.call-update) | async-done | bytes 1048592 | tf_op jit(solution)/shard_map/reduce_scatter | solution.py:69
  176.8 1.9 fusion
  178.7 2.5 all-reduce.1
  181.2 1.5 multiply_convert_fusion.2
  185.0 9.7 %all-gather.14.cloned.1.call-done = bf16[512,2048]{1,0:T(8,128)(2,1)} async-done(((bf16[512,1024]{1,0:T(8,128)(2,1)}), bf16[512,2048]{1,0:T(8,128)(2,1)}) %all-gather.14.cloned.1.call-update) | async-done | bytes 2097168 | tf_op jit(solution)/shard_map/all_gather | solution.py:73
  194.7 145.2 %all-gather.16.cloned.1.call-done = bf16[2048,2816]{1,0:T(8,128)(2,1)} async-done(((bf16[128,2816]{1,0:T(8,128)(2,1)}), bf16[2048,2816]{1,0:T(8,128)(2,1)}) %all-gather.16.cloned.1.call-update) | async-done | bytes 11534352 | tf_op jit(solution)/shard_map/all_gather | solution.py:78
  340.0 12.5 %fusion.38 = f32[512,2816]{1,0:T(8,128)} fusion(bf16[512,2048]{1,0:T(8,128)(2,1)} %all-gather.14.cloned.1.call-done, bf16[2048,2816]{1,0:T(8,128)(2,1)} %all-gather.16.cloned.1.call-done), kind=kOutput, calls=%fused_computation.57 | convolution fusion | flops 5905580032 | bytes 19398656 | tf_op jit(solution)/shard_map/dot_general | solution.py:11
  352.4 130.0 %all-gather.18.cloned.1.call-done = bf16[2048,2816]{1,0:T(8,128)(2,1)} async-done(((bf16[128,2816]{1,0:T(8,128)(2,1)}), bf16[2048,2816]{1,0:T(8,128)(2,1)}) %all-gather.18.cloned.1.call-update) | async-done | bytes 11534352 | tf_op jit(solution)/shard_map/all_gather | solution.py:79
  482.4 183.0 %all-gather.20.cloned.1.call-done = bf16[2816,2048]{1,0:T(8,128)(2,1)} async-done(((bf16[2816,128]{1,0:T(8,128)(2,1)}), bf16[2816,2048]{1,0:T(8,128)(2,1)}) %all-gather.20.cloned.1.call-update) | async-done | bytes 11534352 | tf_op jit(solution)/shard_map/all_gather | solution.py:83
  665.3 22.8 %convolution_convert_fusion = bf16[512,2048]{1,0:T(8,128)(2,1)} fusion(bf16[2816,2048]{1,0:T(8,128)(2,1)} %all-gather.20.cloned.1.call-done, f32[512,2816]{1,0:T(8,128)} %fusion.38, bf16[512,2048]{1,0:T(8,128)(2,1)S(1)} %copy-done.9, bf16[2048,2816]{1,0:T(8,128)(2,1)} %all-gather.18.cloned.1.call-done), kind=kOutput, calls=%fused_computation.1 | convolution fusion | flops 11820859392 | bytes 33030144 | tf_op jit(solution)/shard_map/dot_general | solution.py:81
  688.1 8.0 %reduce-scatter.5.cloned.1.call-done = bf16[512,1024]{1,0:T(8,128)(2,1)} async-done(((bf16[512,2048]{1,0:T(8,128)(2,1)}), bf16[512,1024]{1,0:T(8,128)(2,1)}) %reduce-scatter.5.cloned.1.call-update) | async-done | bytes 1048592 | tf_op jit(solution)/shard_map/reduce_scatter | solution.py:86
  696.1 1.9 fusion.1
  698.0 2.5 all-reduce
  700.5 1.5 multiply_convert_fusion.1
  (45 shorter events, 6.9 us)
Async XLA Ops:
  6.5 15.7 %all-gather.8.cloned.1.call-start = ((), (), s32[]{:S(2)}) async-start(), calls=%async_computation.3 | async-start | bytes 3145728 | tf_op jit(solution)/shard_map/all_gather | solution.py:42
  7.3 90.6 %all-gather.10.cloned.1.call-start = ((), (), s32[]{:S(2)}) async-start(), calls=%async_computation.4 | async-start | bytes 2228224 | tf_op jit(solution)/shard_map/all_gather | solution.py:50
  10.5 99.9 %all-to-all-start = ((bf16[16,128,512]{2,1,0:T(8,128)(2,1)}), bf16[16,128,512]{2,1,0:T(8,128)(2,1)S(1)}, u32[]{:S(2)}, u32[]{:S(2)}) async-start(bf16[16,128,512]{2,1,0:T(8,128)(2,1)} %stack.2), calls=%async_computation | async-start | bytes 4194304 | tf_op jit(solution)/shard_map/all_to_all | solution.py:37
  18.8 143.5 %all-gather.12.cloned.1.call-start = ((), (), s32[]{:S(2)}) async-start(), calls=%async_computation.5 | async-start | bytes 2228224 | tf_op jit(solution)/shard_map/all_gather | solution.py:66
  19.5 157.3 %reduce-scatter.3.cloned.1.call-start = ((), (), s32[]{:S(2)}) async-start(), calls=%async_computation.6 | async-start | bytes 3145728 | tf_op jit(solution)/shard_map/reduce_scatter | solution.py:69
  19.6 85.5 %copy-start.7 = (f32[512]{0:T(512)S(1)}, f32[512]{0:T(512)}, u32[]{:S(2)}) copy-start(f32[512]{0:T(512)} %param.15) | copy-start | bytes 6148
  102.5 5.2 copy-start.4
  102.5 5.2 copy-start.8
  168.8 8.0 %copy-start.1 = (bf16[512,1024]{1,0:T(8,128)(2,1)S(1)}, bf16[512,1024]{1,0:T(8,128)(2,1)}, u32[]{:S(2)}) copy-start(bf16[512,1024]{1,0:T(8,128)(2,1)} %param.12) | copy-start | bytes 3145732
  168.8 12.4 %copy-start.5 = (f32[1024]{0:T(1024)S(1)}, f32[1024]{0:T(1024)}, u32[]{:S(2)}) copy-start(f32[1024]{0:T(1024)} %param.19) | copy-start | bytes 12292
  168.8 25.9 %all-gather.14.cloned.1.call-start = ((), (), s32[]{:S(2)}) async-start(), calls=%async_computation.7 | async-start | bytes 3145728 | tf_op jit(solution)/shard_map/all_gather | solution.py:73
  176.8 4.4 copy-start.2
  182.7 157.2 %all-gather.16.cloned.1.call-start = ((), (), s32[]{:S(2)}) async-start(), calls=%async_computation.8 | async-start | bytes 12255232 | tf_op jit(solution)/shard_map/all_gather | solution.py:78
  183.3 299.1 %all-gather.18.cloned.1.call-start = ((), (), s32[]{:S(2)}) async-start(), calls=%async_computation.9 | async-start | bytes 12255232 | tf_op jit(solution)/shard_map/all_gather | solution.py:79
  184.0 481.3 %all-gather.20.cloned.1.call-start = ((), (), s32[]{:S(2)}) async-start(), calls=%async_computation.10 | async-start | bytes 12255232 | tf_op jit(solution)/shard_map/all_gather | solution.py:83
  184.8 511.3 %reduce-scatter.5.cloned.1.call-start = ((), (), s32[]{:S(2)}) async-start(), calls=%async_computation.11 | async-start | bytes 3145728 | tf_op jit(solution)/shard_map/reduce_scatter | solution.py:86
  194.7 470.6 %copy-start.9 = (bf16[512,2048]{1,0:T(8,128)(2,1)S(1)}, bf16[512,2048]{1,0:T(8,128)(2,1)}, u32[]{:S(2)}) copy-start(bf16[512,2048]{1,0:T(8,128)(2,1)} %all-gather.14.cloned.1.call-done) | copy-start | bytes 6291460
  688.1 8.0 %copy-start = (bf16[512,1024]{1,0:T(8,128)(2,1)S(1)}, bf16[512,1024]{1,0:T(8,128)(2,1)}, u32[]{:S(2)}) copy-start(bf16[512,1024]{1,0:T(8,128)(2,1)} %multiply_convert_fusion.2) | copy-start | bytes 3145732
  688.1 12.4 %copy-start.6 = (f32[1024]{0:T(1024)S(1)}, f32[1024]{0:T(1024)}, u32[]{:S(2)}) copy-start(f32[1024]{0:T(1024)} %param.23) | copy-start | bytes 12292
  696.1 4.4 copy-start.3
Sparse Core Ops, SparseCore 0:
  8.9 13.2 all-gather.7
  25.0 72.8 all-gather.9
  100.6 61.7 all-gather.11
  169.0 7.7 reduce-scatter.2
  182.8 11.8 all-gather.13
  197.3 142.5 all-gather.15
  342.7 139.6 all-gather.17
  485.1 180.2 all-gather.19
  688.3 7.7 reduce-scatter.4
